TPU v7x, 1024 devices: a whole 4x4x32 slice. The times are simulated.
1024 devices in a mesh: gr: 4 (over z_hi), sp: 32 (over z_lo, y), tp: 8 (over x, core).
Axes of the slice: x: 4, y: 4, z: 32 (z_hi: 4, z_lo: 8; z = z_hi * 8 + z_lo), core: 2. Of those that a mesh axis runs over, the one named last changes fastest.
Arguments:
- prompt: bfloat16 [16, 4096, 4096], P('gr', 'sp'), may hold values from -16 to 16
- forget_weight: bfloat16 [4096, 2048], P(None, 'tp'), may hold values from -0.09375 to 0.09375
- value_weight: bfloat16 [4096, 2048], P(None, 'tp'), may hold values from -0.09375 to 0.09375
- leak: float32 [2048], P('tp'), may hold values from 0 to 1, as said below
- query: bfloat16 [16, 2048], P('gr', 'tp'), may hold values from -6 to 6
- next_input: bfloat16 [16, 4096], P('gr'), may hold values from -6 to 6
- read_gain: float32 [2048], P('tp'), may hold values from 0.1 to 1.9
Outputs:
- state_cache: bfloat16 [16, 16, 128, 128], P('gr', 'tp', 'sp')
- read_out: bfloat16 [16, 2048], P('gr', 'tp')
Inputs may be any that keep to these rules, and one draw needn't show every extreme that they name: `leak`: positive, at most one half.
All inputs are finite; a program needn't handle non-finite values.
Results may differ from a plain program's by a relative error of at most 0.0062.
Values sent between devices are 32-bit elements; how exact they have to be, the bound alone decides.
A program may use at most 64 MiB of HBM per device.

v0:
```python
import jax
import jax.numpy as jnp
from jax import lax
from jax.sharding import PartitionSpec as P

DK = 128
DV = 128


def sent_to_all(array, axis):
    count = lax.axis_size(axis)
    return lax.all_to_all(
        jnp.broadcast_to(array[None], (count, *array.shape)), axis, 0, 0, tiled=True
    )


def folded_in_pairs(pieces, combine):
    while len(jax.tree.leaves(pieces)[0]) > 1:
        pieces = jax.vmap(combine)(*(pieces[side::2] for side in (0, 1)))
    return pieces[0]


def entering(array, axis, combine, identity):
    count, index = (lax.axis_size(axis), lax.axis_index(axis))
    passed = jnp.arange(count) > index

    def kept(part, zero, own):
        part = jnp.where(
            passed.reshape(-1, *(1 for _ in own.shape)), part, jnp.asarray(zero, own.dtype)
        )
        return part[::-1]

    pieces = sent_to_all(array, axis)
    return folded_in_pairs(kept(pieces, identity, array), combine)


def in_blocks(array, dim, count):
    before, after = (array.shape[:dim], array.shape[dim + 1 :])
    return jnp.moveaxis(array.reshape(*before, count, -1, *after), dim, 0)


def sum_at_owner(array, axis, dim):
    pieces = in_blocks(array, dim, lax.axis_size(axis))
    arrived = lax.all_to_all(pieces, axis, split_axis=0, concat_axis=0, tiled=True)
    return arrived.sum(axis=0)


def over_copies(array, axis):
    everything = sent_to_all(array, axis)
    return jnp.sum(everything, axis=0)


def add_decay(earlier, later_part):
    return earlier + later_part


def local(prompt, forget_weight, value_weight, leak, query, next_input, read_gain):
    seqs, span, width = prompt.shape
    heads_here = forget_weight.shape[1] // DK
    flat_rows = prompt.reshape(seqs * span, width)
    gate_pre = jnp.dot(flat_rows, forget_weight, preferred_element_type=jnp.float32).reshape(
        seqs, span, heads_here, DK
    )
    values = jnp.dot(flat_rows, value_weight, preferred_element_type=jnp.float32).astype(
        jnp.bfloat16
    )
    values = values.reshape(seqs, span, heads_here, DV)
    leak_heads = leak.reshape(heads_here, DK)
    inflow = leak_heads * jax.nn.sigmoid(-gate_pre)
    seg_cum = jnp.cumsum(jnp.log1p(-inflow), axis=1)
    seg_total = seg_cum[:, -1]
    weighted = (inflow * jnp.exp(seg_total[:, None] - seg_cum)).astype(jnp.bfloat16)
    seg_state = jnp.einsum("sphk,sphv->shkv", weighted, values, preferred_element_type=jnp.float32)
    next_pre = jnp.dot(next_input, forget_weight, preferred_element_type=jnp.float32).reshape(
        seqs, heads_here, DK
    )
    next_values = jnp.dot(next_input, value_weight, preferred_element_type=jnp.float32).astype(
        jnp.bfloat16
    )
    next_values = next_values.astype(jnp.float32).reshape(seqs, heads_here, DV)
    next_inflow = leak_heads * jax.nn.sigmoid(-next_pre)
    next_forget = 1.0 - next_inflow
    queries = query.astype(jnp.float32).reshape(seqs, heads_here, DK)
    rows_here = DK // lax.axis_size("sp")
    start = lax.axis_index("sp") * rows_here
    later = entering(seg_total, "sp", add_decay, jnp.zeros_like(seg_total))
    term = jnp.exp(later)[..., None] * seg_state
    owned = sum_at_owner(term, "sp", 2)
    forget_rows = lax.dynamic_slice_in_dim(next_forget, start, rows_here, 2)
    inflow_rows = lax.dynamic_slice_in_dim(next_inflow, start, rows_here, 2)
    query_rows = lax.dynamic_slice_in_dim(queries, start, rows_here, 2)
    read_rows = forget_rows[..., None] * owned + inflow_rows[..., None] * next_values[:, :, None, :]
    partial_read = jnp.sum(query_rows[..., None] * read_rows, axis=2)
    raw_read = over_copies(partial_read, "sp")
    cache = owned.astype(jnp.bfloat16)
    scaled = raw_read * lax.rsqrt(jnp.mean(raw_read * raw_read, axis=-1, keepdims=True) + 1e-06)
    read_out = (
        (scaled * read_gain.reshape(heads_here, DV))
        .astype(jnp.bfloat16)
        .reshape(seqs, heads_here * DV)
    )
    return (cache, read_out)


def solution(mesh):
    placed = (
        P("gr", "sp", None),
        P(None, "tp"),
        P(None, "tp"),
        P("tp"),
        P("gr", "tp"),
        P("gr", None),
        P("tp"),
    )
    return jax.shard_map(
        local,
        mesh=mesh,
        in_specs=placed,
        out_specs=(P("gr", "tp", "sp", None), P("gr", "tp")),
        check_vma=False,
    )
```

profile of v0, /device:TPU:6, one launch (start us, length us, event | category | flops | bytes accessed | tf_op | source)
XLA Modules:
  0.0 97.7 jit_solution(9187621731918556963)
XLA Ops:
  0.6 0.0 copy-start
  0.6 0.0 copy-start.3
  0.7 4.3 %copy.35 = bf16[256,4096]{1,0:T(8,128)(2,1)} copy(bf16[256,4096]{0,1:T(8,128)(2,1)} %bitcast.45) | data formatting | bytes 4194304 | tf_op jit(solution)/shard_map/dot_general | solution.py:61
  4.9 0.0 copy-done.3
  4.9 4.3 %negate_log-plus-one_fusion = (f32[4,128,2,128]{3,1,2,0:T(8,128)S(1)}, f32[4,128,2,128]{3,1,2,0:T(8,128)S(1)}) fusion(bf16[2,128,4096,1]{2,1,0,3:T(8,128)(2,1)} %bitcast.47, bf16[4,128,4096]{2,1,0:T(8,128)(2,1)} %param.7, f32[2,128]{1,0:T(2,128)S(1)} %bitcast.51), kind=kOutput, calls=%fused_computation.20 | convolution fusion | flops 1074266112 | bytes 7341056 | tf_op jit(solution)/shard_map/dot_general | solution.py:61
  9.2 0.4 fusion.20
  9.7 0.7 broadcast_in_dim.20
  10.4 15.5 %all-to-all-start = ((f32[32,4,2,128]{3,2,1,0:T(2,128)}), f32[32,4,2,128]{3,2,1,0:T(2,128)S(1)}, u32[]{:S(2)}, u32[]{:S(2)}) async-start(f32[32,4,2,128]{3,2,1,0:T(2,128)} %broadcast_in_dim.20), calls=%async_computation | async-start | bytes 262144 | tf_op jit(solution)/shard_map/all_to_all | solution.py:12
  25.9 0.0 copy-done
  25.9 4.1 %convolution_convert_fusion = bf16[512,256]{1,0:T(8,128)(2,1)} fusion(bf16[512,4096]{1,0:T(8,128)(2,1)} %bitcast.53, bf16[4096,256]{1,0:T(8,128)(2,1)S(1)} %copy-done), kind=kOutput, calls=%fused_computation.7 | convolution fusion | flops 1073872896 | bytes 6553600 | tf_op jit(solution)/shard_map/dot_general | solution.py:64
  30.1 1.0 %reshape.64 = bf16[4,128,2,128]{3,2,1,0:T(2,128)(2,1)S(1)} reshape(bf16[512,256]{1,0:T(8,128)(2,1)} %convolution_convert_fusion) | data formatting | bytes 524288 | tf_op jit(solution)/shard_map/reshape | solution.py:67
  31.1 9.1 %all-to-all-done = f32[32,4,2,128]{3,2,1,0:T(2,128)S(1)} async-done(((f32[32,4,2,128]{3,2,1,0:T(2,128)}), f32[32,4,2,128]{3,2,1,0:T(2,128)S(1)}, u32[]{:S(2)}, u32[]{:S(2)}) %all-to-all-start) | async-done | bytes 131104 | tf_op jit(solution)/shard_map/all_to_all | solution.py:12
  40.2 0.1 broadcast_select_fusion
  40.4 0.0 copy-start.1
  40.5 0.3 convolution_multiply_fusion
  40.8 0.0 copy-start.2
  40.8 0.9 copy.52
  41.7 5.0 %all-to-all-start.1 = ((f32[32,4,2,4,128]{4,3,2,1,0:T(4,128)}), f32[32,4,2,4,128]{4,3,2,1,0:T(4,128)S(1)}, u32[]{:S(2)}, u32[]{:S(2)}) async-start(f32[32,4,2,4,128]{4,3,2,1,0:T(4,128)} %bitcast.41), calls=%async_computation.1 | async-start | bytes 1048576 | tf_op jit(solution)/shard_map/all_to_all | solution.py:44
  46.8 0.0 copy-done.1
  46.8 2.0 %fusion.15 = f32[4,256]{1,0:T(4,128)S(1)} fusion(bf16[4,4096]{1,0:T(4,128)(2,1)S(1)} %copy-done.1, bf16[4096,256]{1,0:T(8,128)(2,1)} %param.8), kind=kOutput, calls=%fused_computation.10 | convolution fusion | flops 8390656 | bytes 2134016 | tf_op jit(solution)/shard_map/dot_general | solution.py:74
  48.8 0.0 copy-start.4
  48.8 0.0 copy-done.2
  48.8 0.4 fusion.16
  49.2 0.1 broadcast_subtract_fusion
  49.3 26.7 %all-to-all-done.1 = f32[32,4,2,4,128]{4,3,2,1,0:T(4,128)S(1)} async-done(((f32[32,4,2,4,128]{4,3,2,1,0:T(4,128)}), f32[32,4,2,4,128]{4,3,2,1,0:T(4,128)S(1)}, u32[]{:S(2)}, u32[]{:S(2)}) %all-to-all-start.1) | async-done | bytes 524320 | tf_op jit(solution)/shard_map/all_to_all | solution.py:44
  76.0 0.1 reduce_sum.36
  76.1 0.6 multiply_reduce_fusion
  76.8 20.1 %all_to_all.15 = f32[32,4,2,128]{3,2,1,0:T(2,128)S(1)} all-to-all(f32[32,4,2,128]{3,2,1,0:T(2,128)S(1)} %broadcast_in_dim.35), channel_id=1, replica_groups=mesh['gr'=4,'sp'=32,'tp'=8] {'sp'}, dimensions={0} | all-to-all | bytes 262144 | tf_op jit(solution)/shard_map/all_to_all | solution.py:12
  96.9 0.1 reduce_sum.38
  96.9 0.1 multiply_reduce_fusion.1
  97.0 0.1 multiply_bitcast_fusion
  97.1 0.0 copy-done.4
  97.1 0.6 fusion.25
  (15 shorter events, 0.2 us)
Async XLA Ops:
  0.6 25.3 %copy-start = (bf16[4096,256]{1,0:T(8,128)(2,1)S(1)}, bf16[4096,256]{1,0:T(8,128)(2,1)}, u32[]{:S(2)}) copy-start(bf16[4096,256]{1,0:T(8,128)(2,1)} %param.9) | copy-start | bytes 6291460
  0.6 4.3 %copy-start.3 = (f32[256]{0:T(256)S(1)}, f32[256]{0:T(256)}, u32[]{:S(2)}) copy-start(f32[256]{0:T(256)} %param.10) | copy-start | bytes 3076
  10.4 29.8 %all-to-all-start = ((f32[32,4,2,128]{3,2,1,0:T(2,128)}), f32[32,4,2,128]{3,2,1,0:T(2,128)S(1)}, u32[]{:S(2)}, u32[]{:S(2)}) async-start(f32[32,4,2,128]{3,2,1,0:T(2,128)} %broadcast_in_dim.20), calls=%async_computation | async-start | bytes 262144 | tf_op jit(solution)/shard_map/all_to_all | solution.py:12
  40.4 6.4 %copy-start.1 = (bf16[4,4096]{1,0:T(4,128)(2,1)S(1)}, bf16[4,4096]{1,0:T(4,128)(2,1)}, u32[]{:S(2)}) copy-start(bf16[4,4096]{1,0:T(4,128)(2,1)} %param.12) | copy-start | bytes 98308
  40.8 8.0 %copy-start.2 = (bf16[4,256]{1,0:T(4,128)(2,1)S(1)}, bf16[4,256]{1,0:T(4,128)(2,1)}, u32[]{:S(2)}) copy-start(bf16[4,256]{1,0:T(4,128)(2,1)} %param.11) | copy-start | bytes 6148
  41.7 34.3 %all-to-all-start.1 = ((f32[32,4,2,4,128]{4,3,2,1,0:T(4,128)}), f32[32,4,2,4,128]{4,3,2,1,0:T(4,128)S(1)}, u32[]{:S(2)}, u32[]{:S(2)}) async-start(f32[32,4,2,4,128]{4,3,2,1,0:T(4,128)} %bitcast.41), calls=%async_computation.1 | async-start | bytes 1048576 | tf_op jit(solution)/shard_map/all_to_all | solution.py:44
  48.8 48.3 %copy-start.4 = (f32[256]{0:T(256)S(1)}, f32[256]{0:T(256)}, u32[]{:S(2)}) copy-start(f32[256]{0:T(256)} %param.13) | copy-start | bytes 3076
where the time goes:
time: 98.1 us; the launch traced here: 97.7 us
  waiting for transfers between devices  35.8 us (36%)
  starting transfers between devices  20.6 us (21%)
  blocking collectives  20.1 us (20%)
  matrix products  11.1 us (11%)
  local copies, waits for them, and re-layouts  7.05 us (7%)
  other arithmetic  2.26 us (2%)
    all_to_all x1, waiting for transfers between devices, sum_at_owner(): lax.all_to_all(pieces, axis, split_axis=0, concat_axis=0, tiled=True)  26.7 us
    all_to_all x1, blocking collectives, sent_to_all(): lax.all_to_all(jnp.broadcast_to(array[None], (count, *array.shape)), axis...  20.1 us
    all_to_all x1, starting transfers between devices, sent_to_all(): lax.all_to_all(jnp.broadcast_to(array[None], (count, *array.shape)), axis...  15.5 us
    all_to_all x1, waiting for transfers between devices, sent_to_all(): lax.all_to_all(jnp.broadcast_to(array[None], (count, *array.shape)), axis...  9.08 us
    all_to_all x1, starting transfers between devices, sum_at_owner(): lax.all_to_all(pieces, axis, split_axis=0, concat_axis=0, tiled=True)  5.03 us
    dot_general x1, matrix products, local(): jnp.dot(flat_rows, forget_weight, preferred_element_type=jnp.float32)  4.31 us
    dot_general x1, local copies, waits for them, and re-layouts, local(): jnp.dot(flat_rows, forget_weight, preferred_element_type=jnp.float32)  4.27 us
    dot_general x1, matrix products, local(): jnp.dot(flat_rows, value_weight, preferred_element_type=jnp.float32)  4.13 us
  transfers between devices with their start and end apart: 2, of which 2 were waited for; matrix products, arithmetic and copies ran while one was open for 8% of the time, Pallas kernels for 0%

commit v1 on v0

v1 whole, which is shorter than its diff:
```python
import functools

import jax
import jax.numpy as jnp
from jax import lax
from jax.experimental import pallas as pl
from jax.experimental.pallas import tpu as pltpu
from jax.sharding import PartitionSpec as P

MESH = pl.DeviceIdType.MESH
F32 = jnp.float32
BF16 = jnp.bfloat16
DK = 128
DV = 128
NY = 4
CHUNKS = 4
EPS = 1e-6


def dot(a, b, contract=((1,), (0,))):
    return lax.dot_general(a, b, (contract, ((), ())), preferred_element_type=F32)


def halves(x):
    high = x.astype(BF16)
    return high, (x - high.astype(F32)).astype(BF16)


def kernel(
    nz, prompt, fw, vw, leak_in, query_in, next_in, gain_in, cache_out, read_out,
    x, wf, wv, leak, query, nexts, gain, acc, inflow, decays, vals, packed,
    ys, split, r1, q2, r2, zs, zr, yt, zt, yr, rz, cols, cols_src,
    x_sem, wf_sem, wv_sem, small_sem,
    yt_send, yt_recv, zt_send, zt_recv, r1_send, r1_recv, r2_send, r2_recv,
    zr_send, zr_recv, yr_send, yr_recv, rz_send, rz_recv,
):
    seqs = query.shape[0]
    span = x.shape[0] // seqs
    heads = query.shape[1] // DK
    depth = x.shape[1]
    step = depth // CHUNKS
    me = lax.axis_index("sp")
    z = lax.div(me, NY)
    y = lax.rem(me, NY)

    def at(zz, yy):
        return {"sp": zz * NY + yy}

    y_peers = [lax.rem(y + d, NY) for d in range(1, NY)]
    z_peers = [lax.rem(z + d, nz) for d in range(1, nz)]

    barrier = pltpu.get_barrier_semaphore()
    for p in y_peers:
        pl.semaphore_signal(barrier, inc=1, device_id=at(z, p), device_id_type=MESH)
    for p in z_peers:
        pl.semaphore_signal(barrier, inc=1, device_id=at(p, y), device_id_type=MESH)

    def cut(c):
        return pl.ds(c * step, step)

    x_copies = [pltpu.make_async_copy(prompt.at[:, cut(c)], x.at[:, cut(c)], x_sem.at[c]) for c in range(CHUNKS)]
    f_copies = [pltpu.make_async_copy(fw.at[cut(c)], wf.at[cut(c)], wf_sem.at[c]) for c in range(CHUNKS)]
    v_copies = [pltpu.make_async_copy(vw.at[cut(c)], wv.at[cut(c)], wv_sem.at[c]) for c in range(CHUNKS)]
    small = [
        pltpu.make_async_copy(src, dst, small_sem.at[i])
        for i, (src, dst) in enumerate(((leak_in, leak), (query_in, query), (next_in, nexts), (gain_in, gain)))
    ]
    for c in range(CHUNKS):
        f_copies[c].start()
        x_copies[c].start()
    for copy in small:
        copy.start()

    def remote(src, dst, send, recv, to):
        return pltpu.make_async_remote_copy(
            src_ref=src, dst_ref=dst, send_sem=send, recv_sem=recv, device_id=to, device_id_type=MESH
        )

    for c in range(CHUNKS):
        f_copies[c].wait()
        x_copies[c].wait()
        part = dot(x[:, cut(c)], wf[cut(c), :])
        if c == 0:
            acc[...] = part
            for copy in v_copies:
                copy.start()
        else:
            acc[...] += part
    for copy in small:
        copy.wait()

    leak_row = leak[...]
    totals = []
    for s in range(seqs):
        rows = pl.ds(s * span, span)
        flow = leak_row * jax.nn.sigmoid(-acc[rows, :])
        inflow[rows, :] = flow
        log = jnp.log(1.0 - flow)
        high, low = halves(log)
        decays[s, 0:span, :] = high
        decays[s, span:2 * span, :] = low
        totals.append(jnp.sum(log, axis=0, keepdims=True))

    def by_head(rows):
        return jnp.concatenate([rows[:, h * DK:(h + 1) * DK] for h in range(heads)], axis=0)

    yt[y] = by_head(jnp.concatenate(totals, axis=0))
    pl.semaphore_wait(barrier, NY - 1 + nz - 1)
    yt_copies = [
        remote(yt.at[y], yt.at[y], yt_send.at[i], yt_recv.at[y], at(z, p)) for i, p in enumerate(y_peers)
    ]
    for copy in yt_copies:
        copy.start()

    for c in range(CHUNKS):
        v_copies[c].wait()
        part = dot(x[:, cut(c)], wv[cut(c), :])
        if c == 0:
            acc[...] = part
        elif c < CHUNKS - 1:
            acc[...] += part
        else:
            vals[...] = (acc[...] + part).astype(BF16)

    for p in y_peers:
        remote(yt.at[p], yt.at[p], yt_send.at[0], yt_recv.at[p], at(z, p)).wait_recv()
    all_y = [yt[j] for j in range(NY)]
    later_y = sum(jnp.where(y < j, all_y[j], 0.0) for j in range(1, NY))
    zt[z] = sum(all_y[1:], all_y[0])
    zt_copies = [
        remote(zt.at[z], zt.at[z], zt_send.at[i], zt_recv.at[z], at(p, y)) for i, p in enumerate(z_peers)
    ]
    for copy in zt_copies:
        copy.start()

    rows_at = lax.broadcasted_iota(jnp.int32, (span, 2 * span), 0)
    cols_at = lax.rem(lax.broadcasted_iota(jnp.int32, (span, 2 * span), 1), span)
    upper = jnp.where(cols_at > rows_at, 1.0, 0.0).astype(BF16)

    first, second = [], []
    for s in range(seqs):
        pair = y + 1 - 2 * lax.rem(y, 2)
        across = NY - 1 - y
        first.append(pair if s % 2 == 0 else across)
        second.append(across if s % 2 == 0 else pair)

    r1_copies = []
    for s in range(seqs):
        rows = pl.ds(s * span, span)
        later_row = jnp.concatenate([later_y[h * seqs + s:h * seqs + s + 1, :] for h in range(heads)], axis=1)
        left = dot(upper, decays[s]) + later_row
        weighted = (inflow[rows, :] * jnp.exp(left)).astype(BF16)
        for h in range(heads):
            lanes = slice(h * DK, (h + 1) * DK)
            state = dot(weighted[:, lanes], vals[rows, lanes], ((0,), (0,)))
            high, low = halves(state)
            split[s, 0:DK, lanes] = high
            split[s, DK:2 * DK, lanes] = low
            own = DK // (NY * nz)
            for zz in range(nz):
                for yy in range(NY):
                    k = (zz * NY + yy) * own
                    ys[yy, s, zz, h * own:(h + 1) * own, :] = state[k:k + own, :]
        p = first[s]
        beyond = NY - 1 - p if s % 2 == 0 else p + 1 - 2 * lax.rem(p, 2)
        for i, target in enumerate((beyond, p)):
            copy = remote(ys.at[target, s], r1.at[s, 1 - i], r1_send.at[s, i], r1_recv.at[s, 1 - i], at(z, p))
            copy.start()
            r1_copies.append(copy)

    forget_pre, next_vals = None, None
    for c in range(CHUNKS):
        piece = nexts[:, cut(c)]
        a, b = dot(piece, wf[cut(c), :]), dot(piece, wv[cut(c), :])
        forget_pre = a if c == 0 else forget_pre + a
        next_vals = b if c == 0 else next_vals + b
    next_flow = leak_row * jax.nn.sigmoid(-forget_pre)
    queries = query[...].astype(F32)
    through = by_head(queries * (1.0 - next_flow))
    direct = jnp.sum(by_head(queries * next_flow), axis=1, keepdims=True) * by_head(
        next_vals.astype(BF16).astype(F32)
    )

    r2_copies = []
    for s in range(seqs):
        r1_copies[2 * s].wait_recv()
        q2[s] = ys[second[s], s] + r1[s, 1]
        copy = remote(q2.at[s], r2.at[s], r2_send.at[s], r2_recv.at[s], at(z, second[s]))
        copy.start()
        r2_copies.append(copy)

    for p in z_peers:
        remote(zt.at[p], zt.at[p], zt_send.at[0], zt_recv.at[p], at(p, y)).wait_recv()
    running = jnp.zeros_like(through)
    later_z = jnp.zeros_like(through)
    for j in reversed(range(nz)):
        cols_src[j * seqs * heads:(j + 1) * seqs * heads, :] = jnp.exp(running)
        later_z = jnp.where(z == j, running, later_z)
        running = running + zt[j]
    weights = through * jnp.exp(later_z)
    high, low = halves(weights)
    packed[...] = jnp.concatenate([jnp.concatenate([high, low], axis=0)] * 2, axis=1)
    units = seqs * heads
    parts = [None] * units
    for s in range(seqs):
        got = dot(packed[...], split[s])
        for h in range(heads):
            u = h * seqs + s
            lanes = slice(h * DK, (h + 1) * DK)
            parts[u] = got[u:u + 1, lanes] + got[units + u:units + u + 1, lanes]
    yr[y] = jnp.concatenate(parts, axis=0)
    yr_copies = [
        remote(yr.at[y], yr.at[y], yr_send.at[i], yr_recv.at[y], at(z, p)) for i, p in enumerate(y_peers)
    ]
    for copy in yr_copies:
        copy.start()

    zr_copies = []
    for s in range(seqs):
        r1_copies[2 * s + 1].wait_recv()
        r2_copies[s].wait_recv()
        zs[s] = ys[y, s] + r1[s, 0] + r2[s]
        for i, p in enumerate(z_peers):
            copy = remote(zs.at[s, p], zr.at[z, s], zr_send.at[s, i], zr_recv.at[z, s], at(p, y))
            copy.start()
            zr_copies.append(copy)
        zr[z, s] = zs[s, z]

    for p in y_peers:
        remote(yr.at[p], yr.at[p], yr_send.at[0], yr_recv.at[p], at(z, p)).wait_recv()
    rz[z] = (yr[0] + yr[1]) + (yr[2] + yr[3])
    rz_copies = [
        remote(rz.at[z], rz.at[z], rz_send.at[i], rz_recv.at[z], at(p, y)) for i, p in enumerate(z_peers)
    ]
    for copy in rz_copies:
        copy.start()

    own = DK // (NY * nz)
    cols[...] = jnp.transpose(cols_src[...])
    mine = cols[pl.ds(me * own, own), :]

    def column(j, s):
        one = [
            jnp.broadcast_to(mine[:, c:c + 1], (own, DV))
            for c in (j * units + h * seqs + s for h in range(heads))
        ]
        return jnp.concatenate(one, axis=0)

    scale = [[column(j, s) for s in range(seqs)] for j in range(nz)]
    for p in z_peers:
        for s in range(seqs):
            remote(zr.at[p, s], zr.at[p, s], zr_send.at[0, 0], zr_recv.at[p, s], at(p, y)).wait_recv()
    for s in range(seqs):
        total = scale[0][s] * zr[0, s]
        for j in range(1, nz):
            total = total + scale[j][s] * zr[j, s]
        cache_out[s] = total.astype(BF16)

    for p in z_peers:
        remote(rz.at[p], rz.at[p], rz_send.at[0], rz_recv.at[p], at(p, y)).wait_recv()
    raw = direct
    for j in range(nz):
        raw = raw + rz[j]
    gain_row = gain[...]
    gains = jnp.concatenate(
        [jnp.broadcast_to(gain_row[:, h * DV:(h + 1) * DV], (seqs, DV)) for h in range(heads)], axis=0
    )
    normed = raw * lax.rsqrt(jnp.mean(raw * raw, axis=1, keepdims=True) + EPS) * gains
    read_out[...] = jnp.concatenate(
        [normed[h * seqs:(h + 1) * seqs, :] for h in range(heads)], axis=1
    ).astype(BF16)

    for copy in yt_copies + zt_copies + r1_copies + r2_copies + zr_copies + yr_copies + rz_copies:
        copy.wait_send()


def local(prompt, forget_weight, value_weight, leak, query, next_input, read_gain):
    seqs, span, depth = prompt.shape
    width = forget_weight.shape[1]
    heads = width // DK
    nz = lax.axis_size("sp") // NY
    own = DK // (NY * nz)
    units = seqs * heads
    dma = pltpu.SemaphoreType.DMA
    anywhere = pl.BlockSpec(memory_space=pl.ANY)
    cache, read = pl.pallas_call(
        functools.partial(kernel, nz),
        out_shape=(
            jax.ShapeDtypeStruct((seqs, heads * own, DV), BF16),
            jax.ShapeDtypeStruct((seqs, width), BF16),
        ),
        in_specs=[anywhere] * 7,
        out_specs=(pl.BlockSpec(memory_space=pltpu.VMEM), pl.BlockSpec(memory_space=pltpu.VMEM)),
        scratch_shapes=[
            pltpu.VMEM((seqs * span, depth), BF16),
            pltpu.VMEM((depth, width), BF16),
            pltpu.VMEM((depth, width), BF16),
            pltpu.VMEM((1, width), F32),
            pltpu.VMEM((seqs, width), BF16),
            pltpu.VMEM((seqs, depth), BF16),
            pltpu.VMEM((1, width), F32),
            pltpu.VMEM((seqs * span, width), F32),
            pltpu.VMEM((seqs * span, width), F32),
            pltpu.VMEM((seqs, 2 * span, width), BF16),
            pltpu.VMEM((seqs * span, width), BF16),
            pltpu.VMEM((2 * units, 2 * DK), BF16),
            pltpu.VMEM((NY, seqs, nz, heads * own, DV), F32),
            pltpu.VMEM((seqs, 2 * DK, width), BF16),
            pltpu.VMEM((seqs, 2, nz, heads * own, DV), F32),
            pltpu.VMEM((seqs, nz, heads * own, DV), F32),
            pltpu.VMEM((seqs, nz, heads * own, DV), F32),
            pltpu.VMEM((seqs, nz, heads * own, DV), F32),
            pltpu.VMEM((nz, seqs, heads * own, DV), F32),
            pltpu.VMEM((NY, units, DK), F32),
            pltpu.VMEM((nz, units, DK), F32),
            pltpu.VMEM((NY, units, DV), F32),
            pltpu.VMEM((nz, units, DV), F32),
            pltpu.VMEM((DK, nz * units), F32),
            pltpu.VMEM((nz * units, DK), F32),
            dma((CHUNKS,)),
            dma((CHUNKS,)),
            dma((CHUNKS,)),
            dma((4,)),
            dma((NY - 1,)),
            dma((NY,)),
            dma((nz - 1,)),
            dma((nz,)),
            dma((seqs, 2)),
            dma((seqs, 2)),
            dma((seqs,)),
            dma((seqs,)),
            dma((seqs, nz - 1)),
            dma((nz, seqs)),
            dma((NY - 1,)),
            dma((NY,)),
            dma((nz - 1,)),
            dma((nz,)),
        ],
        compiler_params=pltpu.CompilerParams(
            collective_id=0, has_side_effects=True, vmem_limit_bytes=60 * 1024 * 1024
        ),
    )(
        prompt.reshape(seqs * span, depth),
        forget_weight,
        value_weight,
        leak.reshape(1, width),
        query,
        next_input,
        read_gain.reshape(1, width),
    )
    return cache.reshape(seqs, heads, own, DV), read


def solution(mesh):
    placed = (
        P("gr", "sp", None),
        P(None, "tp"),
        P(None, "tp"),
        P("tp"),
        P("gr", "tp"),
        P("gr", None),
        P("tp"),
    )
    return jax.shard_map(
        local,
        mesh=mesh,
        in_specs=placed,
        out_specs=(P("gr", "tp", "sp", None), P("gr", "tp")),
        check_vma=False,
    )
```

time: 98.1 us -> 41.5 us (0.42)
  the two profiles are of different devices: /device:TPU:6 before, /device:TPU:8 now
where the time goes in v1:
time: 41.5 us; the launch traced here: 41.2 us
  Pallas kernels  38.1 us (92%)
  local copies, waits for them, and re-layouts  2.53 us (6%)
  between operations  0.64 us (2%)
    pallas_call x1, Pallas kernels, local(): pl.pallas_call(functools.partial(kernel, nz), out_shape=(jax.ShapeDtypeSt...  38.1 us
    unnamed x2, local copies, waits for them, and re-layouts  2.53 us

profile of v1, /device:TPU:8, one launch (start us, length us, event | category | flops | bytes accessed | tf_op | source)
XLA Modules:
  0.0 41.2 jit_solution(17440919707578482982)
XLA Ops:
  0.6 38.1 %shard_map.86 = (bf16[4,8,128]{2,1,0:T(8,128)(2,1)}, bf16[4,256]{1,0:T(4,128)(2,1)}) custom-call(bf16[512,4096]{1,0:T(8,128)(2,1)} %bitcast.4, bf16[4096,256]{1,0:T(8,128)(2,1)} %fw.1, bf16[4096,256]{1,0:T(8,128)(2,1)} %vw.1, f32[1,256]{1,0:T(1,128)} %bitcast.6, bf16[4,256]{1,0:T(4,128)(2,1)} %query_in.1, bf16[4,4096]{1,0:T(4,128)(2,1)} %next_in.1, ...), custom_call_target="tpu_custom_call" | custom-call | tf_op jit(solution)/shard_map/pallas_call | solution.py:286
  38.7 1.3 %copy.11 = bf16[4,2,4,128]{3,2,1,0:T(4,128)(2,1)} copy(bf16[4,2,4,128]{3,2,1,0:T(4,128)(2,1)} %bitcast.5) | data formatting | bytes 16384
  40.0 1.2 %copy.12 = bf16[4,256]{1,0:T(4,128)(2,1)} copy(bf16[4,256]{1,0:T(4,128)(2,1)} %get-tuple-element.9) | data formatting | bytes 4096

commit v2 on v1

v2 whole, which is shorter than its diff:
```python
import functools

import jax
import jax.numpy as jnp
from jax import lax
from jax.experimental import pallas as pl
from jax.experimental.pallas import tpu as pltpu
from jax.sharding import PartitionSpec as P

MESH = pl.DeviceIdType.MESH
F32 = jnp.float32
BF16 = jnp.bfloat16
DK = 128
DV = 128
NY = 4
CHUNKS = 8
EPS = 1e-6


def dot(a, b, contract=((1,), (0,))):
    return lax.dot_general(a, b, (contract, ((), ())), preferred_element_type=F32)


def halves(x):
    high = x.astype(BF16)
    return high, (x - high.astype(F32)).astype(BF16)


def kernel(
    nz, prompt, fw, vw, leak_in, query_in, next_in, gain_in, cache_out, read_out,
    x, w, leak, query, nexts, gain, acc, inflow, decays, packed,
    ys, split, r1, q2, r2, zs, zr, yt, zt, yr, rz, cols, cols_src, near, near_src,
    load_sem, small_sem,
    yt_send, yt_recv, zt_send, zt_recv, r1_send, r1_recv, r2_send, r2_recv,
    zr_send, zr_recv, yr_send, yr_recv, rz_send, rz_recv,
):
    seqs = query.shape[0]
    span = x.shape[0] // seqs
    width = query.shape[1]
    heads = width // DK
    depth = x.shape[1]
    step = depth // CHUNKS
    me = lax.axis_index("sp")
    z = lax.div(me, NY)
    y = lax.rem(me, NY)

    def at(zz, yy):
        return {"sp": zz * NY + yy}

    y_peers = [lax.rem(y + d, NY) for d in range(1, NY)]
    z_peers = [lax.rem(z + d, nz) for d in range(1, nz)]

    barrier = pltpu.get_barrier_semaphore()
    for p in y_peers:
        pl.semaphore_signal(barrier, inc=1, device_id=at(z, p), device_id_type=MESH)
    for p in z_peers:
        pl.semaphore_signal(barrier, inc=1, device_id=at(p, y), device_id_type=MESH)

    def cut(c):
        return pl.ds(c * step, step)

    x_copies = [pltpu.make_async_copy(prompt.at[:, cut(c)], x.at[:, cut(c)], load_sem.at[c]) for c in range(CHUNKS)]
    f_copies = [pltpu.make_async_copy(fw.at[cut(c)], w.at[cut(c), 0:width], load_sem.at[c]) for c in range(CHUNKS)]
    v_copies = [pltpu.make_async_copy(vw.at[cut(c)], w.at[cut(c), width:2 * width], load_sem.at[c]) for c in range(CHUNKS)]
    small = [
        pltpu.make_async_copy(src, dst, small_sem.at[i])
        for i, (src, dst) in enumerate(((leak_in, leak), (query_in, query), (next_in, nexts), (gain_in, gain)))
    ]
    for c in range(CHUNKS):
        f_copies[c].start()
        x_copies[c].start()
        v_copies[c].start()
    for copy in small:
        copy.start()

    def remote(src, dst, send, recv, to):
        return pltpu.make_async_remote_copy(
            src_ref=src, dst_ref=dst, send_sem=send, recv_sem=recv, device_id=to, device_id_type=MESH
        )

    def arrive(ref, sem):
        pltpu.make_async_copy(ref, ref, sem).wait()

    for c in range(CHUNKS):
        arrive(w.at[0:2 * step], load_sem.at[c])
        part = dot(x[:, cut(c)], w[cut(c), :])
        if c == 0:
            acc[...] = part
        else:
            acc[...] += part
    for copy in small:
        copy.wait()

    leak_row = leak[...]
    totals = []
    for s in range(seqs):
        rows = pl.ds(s * span, span)
        flow = leak_row * jax.nn.sigmoid(-acc[rows, 0:width])
        inflow[rows, :] = flow
        log = jnp.log(1.0 - flow)
        high, low = halves(log)
        decays[s, 0:span, :] = high
        decays[s, span:2 * span, :] = low
        totals.append(jnp.sum(log, axis=0, keepdims=True))

    def by_head(rows):
        return jnp.concatenate([rows[:, h * DK:(h + 1) * DK] for h in range(heads)], axis=0)

    yt[y] = by_head(jnp.concatenate(totals, axis=0))
    pl.semaphore_wait(barrier, NY - 1 + nz - 1)
    yt_copies = [
        remote(yt.at[y], yt.at[y], yt_send, yt_recv, at(z, p)) for i, p in enumerate(y_peers)
    ]
    for copy in yt_copies:
        copy.start()

    rows_at = lax.broadcasted_iota(jnp.int32, (span, 2 * span), 0)
    cols_at = lax.rem(lax.broadcasted_iota(jnp.int32, (span, 2 * span), 1), span)
    own = DK // (NY * nz)
    upper = jnp.where(cols_at > rows_at, 1.0, 0.0).astype(BF16)

    pair = y + 1 - 2 * lax.rem(y, 2)
    across = NY - 1 - y
    first, second = [], []
    for s in range(seqs):
        first.append(pair if s % 2 == 0 else across)
        second.append(across if s % 2 == 0 else pair)

    far_copies, near_copies = [], []
    for s in range(seqs):
        rows = pl.ds(s * span, span)
        left = dot(upper, decays[s])
        vals = acc[rows, width:2 * width].astype(BF16)
        weighted = (inflow[rows, :] * jnp.exp(left)).astype(BF16)
        for h in range(heads):
            lanes = slice(h * DK, (h + 1) * DK)
            state = dot(weighted[:, lanes], vals[:, lanes], ((0,), (0,)))
            high, low = halves(state)
            split[s, 0:DK, lanes] = high
            split[s, DK:2 * DK, lanes] = low
            for zz in range(nz):
                for yy in range(NY):
                    k = (zz * NY + yy) * own
                    ys[yy, s, zz, h * own:(h + 1) * own, :] = state[k:k + own, :]
        p = first[s]
        beyond = NY - 1 - p if s % 2 == 0 else p + 1 - 2 * lax.rem(p, 2)
        copy = remote(ys.at[beyond, s], r1.at[s, 1], r1_send, r1_recv.at[s, 1], at(z, p))
        copy.start()
        far_copies.append(copy)
    for s in range(seqs):
        p = first[s]
        copy = remote(ys.at[p, s], r1.at[s, 0], r1_send, r1_recv.at[s, 0], at(z, p))
        copy.start()
        near_copies.append(copy)

    for c in range(CHUNKS):
        part = dot(nexts[:, cut(c)], w[cut(c), :])
        next_pre = part if c == 0 else next_pre + part
    forget_pre, next_vals = next_pre[:, 0:width], next_pre[:, width:2 * width]
    next_flow = leak_row * jax.nn.sigmoid(-forget_pre)
    queries = query[...].astype(F32)
    through = by_head(queries * (1.0 - next_flow))
    direct = jnp.sum(by_head(queries * next_flow), axis=1, keepdims=True) * by_head(
        next_vals.astype(BF16).astype(F32)
    )

    arrive(yt.at[0:NY - 1], yt_recv)
    all_y = [yt[j] for j in range(NY)]
    zt[z] = sum(all_y[1:], all_y[0])
    zt_copies = [
        remote(zt.at[z], zt.at[z], zt_send, zt_recv.at[z], at(p, y)) for i, p in enumerate(z_peers)
    ]
    for copy in zt_copies:
        copy.start()

    def after(p):
        return jnp.exp(sum(jnp.where(p < j, all_y[j], 0.0) for j in range(1, NY)))

    units = seqs * heads
    here = after(y)
    near_src[0:units, :] = here
    near_src[units:2 * units, :] = after(pair)
    near_src[2 * units:3 * units, :] = after(across)
    near_src[3 * units:4 * units, :] = jnp.zeros_like(here)
    near[...] = jnp.transpose(near_src[...])

    def spread(rows, lanes):
        return jnp.concatenate([jnp.broadcast_to(rows[:, c:c + 1], (own, DV)) for c in lanes], axis=0)

    def near_scale(target, which, s):
        return [
            spread(near[pl.ds((j * NY + target) * own, own), :], [which * units + h * seqs + s for h in range(heads)])
            for j in range(nz)
        ]

    r2_copies = []
    for s in range(seqs):
        mine, theirs = near_scale(second[s], 0, s), near_scale(second[s], 1 + s % 2, s)
        far_copies[s].wait_recv()
        for j in range(nz):
            q2[s, j] = mine[j] * ys[second[s], s, j] + theirs[j] * r1[s, 1, j]
        copy = remote(q2.at[s], r2.at[s], r2_send, r2_recv.at[s], at(z, second[s]))
        copy.start()
        r2_copies.append(copy)

    zr_copies = []
    for s in range(seqs):
        mine, theirs = near_scale(y, 0, s), near_scale(y, 1 + s % 2, s)
        near_copies[s].wait_recv()
        r2_copies[s].wait_recv()
        for j in range(nz):
            zs[s, j] = (mine[j] * ys[y, s, j] + theirs[j] * r1[s, 0, j]) + r2[s, j]
        for i, p in enumerate(z_peers):
            copy = remote(zs.at[s, p], zr.at[z, s], zr_send, zr_recv.at[s], at(p, y))
            copy.start()
            zr_copies.append(copy)
        zr[z, s] = zs[s, z]

    def add_later(j, total):
        arrive(zt.at[j], zt_recv.at[j])
        return total + zt[j]

    later_z = lax.fori_loop(z + 1, nz, add_later, jnp.zeros_like(through))
    weights = through * here * jnp.exp(later_z)
    high, low = halves(weights)
    packed[...] = jnp.concatenate([jnp.concatenate([high, low], axis=0)] * 2, axis=1)
    parts = [None] * units
    for s in range(seqs):
        got = dot(packed[...], split[s])
        for h in range(heads):
            u = h * seqs + s
            lanes = slice(h * DK, (h + 1) * DK)
            parts[u] = got[u:u + 1, lanes] + got[units + u:units + u + 1, lanes]
    yr[y] = jnp.concatenate(parts, axis=0)
    yr_copies = [
        remote(yr.at[y], yr.at[y], yr_send, yr_recv, at(z, p)) for i, p in enumerate(y_peers)
    ]
    for copy in yr_copies:
        copy.start()

    arrive(yr.at[0:NY - 1], yr_recv)
    rz[z] = (yr[0] + yr[1]) + (yr[2] + yr[3])
    rz_copies = [
        remote(rz.at[z], rz.at[z], rz_send, rz_recv, at(p, y)) for i, p in enumerate(z_peers)
    ]
    for copy in rz_copies:
        copy.start()

    def await_rest(j, carry):
        arrive(zt.at[j], zt_recv.at[j])
        return carry

    lax.fori_loop(0, z, await_rest, 0)
    running = jnp.zeros_like(through)
    for j in reversed(range(nz)):
        cols_src[j * units:(j + 1) * units, :] = jnp.exp(running)
        running = running + zt[j]
    cols[...] = jnp.transpose(cols_src[...])
    mine = cols[pl.ds(me * own, own), :]

    def column(j, s):
        return spread(mine, [j * units + h * seqs + s for h in range(heads)])

    scale = [[column(j, s) for s in range(seqs)] for j in range(nz)]
    for s in range(seqs):
        arrive(zr.at[0:nz - 1, s], zr_recv.at[s])
    for s in range(seqs):
        total = scale[0][s] * zr[0, s]
        for j in range(1, nz):
            total = total + scale[j][s] * zr[j, s]
        cache_out[s] = total.astype(BF16)

    arrive(rz.at[0:nz - 1], rz_recv)
    raw = direct
    for j in range(nz):
        raw = raw + rz[j]
    gain_row = gain[...]
    gains = jnp.concatenate(
        [jnp.broadcast_to(gain_row[:, h * DV:(h + 1) * DV], (seqs, DV)) for h in range(heads)], axis=0
    )
    normed = raw * lax.rsqrt(jnp.mean(raw * raw, axis=1, keepdims=True) + EPS) * gains
    read_out[...] = jnp.concatenate(
        [normed[h * seqs:(h + 1) * seqs, :] for h in range(heads)], axis=1
    ).astype(BF16)

    arrive(yt.at[0:NY - 1], yt_send)
    arrive(zt.at[0:nz - 1], zt_send)
    for i in range(2):
        arrive(r1.at[:, i], r1_send)
    arrive(r2, r2_send)
    arrive(zr.at[0:nz - 1], zr_send)
    arrive(yr.at[0:NY - 1], yr_send)
    arrive(rz.at[0:nz - 1], rz_send)


def local(prompt, forget_weight, value_weight, leak, query, next_input, read_gain):
    seqs, span, depth = prompt.shape
    width = forget_weight.shape[1]
    heads = width // DK
    nz = lax.axis_size("sp") // NY
    own = DK // (NY * nz)
    units = seqs * heads
    dma = pltpu.SemaphoreType.DMA
    anywhere = pl.BlockSpec(memory_space=pl.ANY)
    cache, read = pl.pallas_call(
        functools.partial(kernel, nz),
        out_shape=(
            pltpu.VMEM((seqs, heads * own, DV), BF16),
            pltpu.VMEM((seqs, width), BF16),
        ),
        in_specs=[anywhere] * 7,
        out_specs=(pl.BlockSpec(memory_space=pltpu.VMEM), pl.BlockSpec(memory_space=pltpu.VMEM)),
        scratch_shapes=[
            pltpu.VMEM((seqs * span, depth), BF16),
            pltpu.VMEM((depth, 2 * width), BF16),
            pltpu.VMEM((1, width), F32),
            pltpu.VMEM((seqs, width), BF16),
            pltpu.VMEM((seqs, depth), BF16),
            pltpu.VMEM((1, width), F32),
            pltpu.VMEM((seqs * span, 2 * width), F32),
            pltpu.VMEM((seqs * span, width), F32),
            pltpu.VMEM((seqs, 2 * span, width), BF16),
            pltpu.VMEM((2 * units, 2 * DK), BF16),
            pltpu.VMEM((NY, seqs, nz, heads * own, DV), F32),
            pltpu.VMEM((seqs, 2 * DK, width), BF16),
            pltpu.VMEM((seqs, 2, nz, heads * own, DV), F32),
            pltpu.VMEM((seqs, nz, heads * own, DV), F32),
            pltpu.VMEM((seqs, nz, heads * own, DV), F32),
            pltpu.VMEM((seqs, nz, heads * own, DV), F32),
            pltpu.VMEM((nz, seqs, heads * own, DV), F32),
            pltpu.VMEM((NY, units, DK), F32),
            pltpu.VMEM((nz, units, DK), F32),
            pltpu.VMEM((NY, units, DV), F32),
            pltpu.VMEM((nz, units, DV), F32),
            pltpu.VMEM((DK, nz * units), F32),
            pltpu.VMEM((nz * units, DK), F32),
            pltpu.VMEM((DK, 4 * units), F32),
            pltpu.VMEM((4 * units, DK), F32),
            dma((CHUNKS,)),
            dma((4,)),
            dma,
            dma,
            dma,
            dma((nz,)),
            dma,
            dma((seqs, 2)),
            dma,
            dma((seqs,)),
            dma,
            dma((seqs,)),
            dma,
            dma,
            dma,
            dma,
        ],
        compiler_params=pltpu.CompilerParams(
            collective_id=0, has_side_effects=True, vmem_limit_bytes=60 * 1024 * 1024
        ),
    )(
        prompt.reshape(seqs * span, depth),
        forget_weight,
        value_weight,
        leak.reshape(1, width),
        query,
        next_input,
        read_gain.reshape(1, width),
    )
    return cache.reshape(seqs, heads, own, DV), read


def solution(mesh):
    placed = (
        P("gr", "sp", None),
        P(None, "tp"),
        P(None, "tp"),
        P("tp"),
        P("gr", "tp"),
        P("gr", None),
        P("tp"),
    )
    return jax.shard_map(
        local,
        mesh=mesh,
        in_specs=placed,
        out_specs=(P("gr", "tp", "sp", None), P("gr", "tp")),
        check_vma=False,
    )
```

time: 41.5 us -> 36.1 us (0.87)
  Pallas kernels: 38.1 us -> 34.1 us
  local copies, waits for them, and re-layouts: 2.53 us -> 1.18 us
    pallas_call x1, Pallas kernels: 38.1 us -> 34.1 us  [local(): pl.pallas_call(functools.partial(kernel, nz), out_shape=(pltpu.VMEM((seqs...]
    unnamed x2, local copies, waits for them, and re-layouts: 2.53 us -> 1.18 us
where the time goes in v2:
time: 36.1 us; the launch traced here: 35.9 us
  Pallas kernels  34.1 us (94%)
  local copies, waits for them, and re-layouts  1.18 us (3%)
  between operations  0.64 us (2%)
    pallas_call x1, Pallas kernels, local(): pl.pallas_call(functools.partial(kernel, nz), out_shape=(pltpu.VMEM((seqs...  34.1 us
    unnamed x2, local copies, waits for them, and re-layouts  1.18 us

profile of v2, /device:TPU:8, one launch (start us, length us, event | category | flops | bytes accessed | tf_op | source)
XLA Modules:
  0.0 35.9 jit_solution(13486174106589217780)
XLA Ops:
  0.6 34.1 %shard_map.86 = (bf16[4,8,128]{2,1,0:T(8,128)(2,1)S(1)}, bf16[4,256]{1,0:T(4,128)(2,1)S(1)}) custom-call(bf16[512,4096]{1,0:T(8,128)(2,1)} %bitcast.5, bf16[4096,256]{1,0:T(8,128)(2,1)} %fw.1, bf16[4096,256]{1,0:T(8,128)(2,1)} %vw.1, f32[1,256]{1,0:T(1,128)} %bitcast.6, bf16[4,256]{1,0:T(4,128)(2,1)} %query_in.1, bf16[4,4096]{1,0:T(4,128)(2,1)} %next_in.1, ...), custom_call_target="tpu_custom_call" | custom-call | tf_op jit(solution)/shard_map/pallas_call | solution.py:305
  34.8 0.6 %copy.11 = bf16[4,2,4,128]{3,2,1,0:T(4,128)(2,1)} copy(bf16[4,2,4,128]{3,2,1,0:T(4,128)(2,1)S(1)} %bitcast.4) | data formatting | bytes 16384
  35.4 0.6 %copy.12 = bf16[4,256]{1,0:T(4,128)(2,1)} copy(bf16[4,256]{1,0:T(4,128)(2,1)S(1)} %get-tuple-element.7) | data formatting | bytes 4096

commit v3 on v2

--- a/solution.py
+++ b/solution.py
@@ -30,7 +30,7 @@
     nz, prompt, fw, vw, leak_in, query_in, next_in, gain_in, cache_out, read_out,
     x, w, leak, query, nexts, gain, acc, inflow, decays, packed,
     ys, split, r1, q2, r2, zs, zr, yt, zt, yr, rz, cols, cols_src, near, near_src,
-    load_sem, small_sem,
+    load_sem, small_sem, corner_in,
     yt_send, yt_recv, zt_send, zt_recv, r1_send, r1_recv, r2_send, r2_recv,
     zr_send, zr_recv, yr_send, yr_recv, rz_send, rz_recv,
 ):
@@ -48,13 +48,17 @@
         return {"sp": zz * NY + yy}
 
     y_peers = [lax.rem(y + d, NY) for d in range(1, NY)]
-    z_peers = [lax.rem(z + d, nz) for d in range(1, nz)]
+    z_peers = [1 + lax.rem(z + i - 1, nz - 1) for i in range(1, nz - 1)]
+    z_peers.append((nz - 1) * lax.div(nz - z, nz))
 
     barrier = pltpu.get_barrier_semaphore()
     for p in y_peers:
         pl.semaphore_signal(barrier, inc=1, device_id=at(z, p), device_id_type=MESH)
-    for p in z_peers:
-        pl.semaphore_signal(barrier, inc=1, device_id=at(p, y), device_id_type=MESH)
+
+    @pl.when(me > 0)
+    def _():
+        for p in z_peers:
+            pl.semaphore_signal(barrier, inc=1, device_id=at(p, y), device_id_type=MESH)
 
     def cut(c):
         return pl.ds(c * step, step)
@@ -73,6 +77,15 @@
     for copy in small:
         copy.start()
 
+    def greet_column():
+        pl.semaphore_wait(barrier, NY - 1 + nz - 1)
+        for p in z_peers:
+            pl.semaphore_signal(corner_in, inc=1, device_id=at(p, y), device_id_type=MESH)
+
+    corner = me == 0
+    early = corner & (lax.axis_index("gr") == 0) & (lax.axis_index("tp") == 0)
+    pl.when(early)(greet_column)
+
     def remote(src, dst, send, recv, to):
         return pltpu.make_async_remote_copy(
             src_ref=src, dst_ref=dst, send_sem=send, recv_sem=recv, device_id=to, device_id_type=MESH
@@ -107,7 +120,17 @@
         return jnp.concatenate([rows[:, h * DK:(h + 1) * DK] for h in range(heads)], axis=0)
 
     yt[y] = by_head(jnp.concatenate(totals, axis=0))
-    pl.semaphore_wait(barrier, NY - 1 + nz - 1)
+    pl.when(corner & jnp.logical_not(early))(greet_column)
+    under = (y == 0) & (z > 0)
+
+    @pl.when(under)
+    def _():
+        pl.semaphore_wait(barrier, NY - 1 + nz - 2)
+
+    @pl.when(y > 0)
+    def _():
+        pl.semaphore_wait(barrier, NY - 1 + nz - 1)
+
     yt_copies = [
         remote(yt.at[y], yt.at[y], yt_send, yt_recv, at(z, p)) for i, p in enumerate(y_peers)
     ]
@@ -142,6 +165,7 @@
                 for yy in range(NY):
                     k = (zz * NY + yy) * own
                     ys[yy, s, zz, h * own:(h + 1) * own, :] = state[k:k + own, :]
+    for s in range(seqs):
         p = first[s]
         beyond = NY - 1 - p if s % 2 == 0 else p + 1 - 2 * lax.rem(p, 2)
         copy = remote(ys.at[beyond, s], r1.at[s, 1], r1_send, r1_recv.at[s, 1], at(z, p))
@@ -170,8 +194,14 @@
     zt_copies = [
         remote(zt.at[z], zt.at[z], zt_send, zt_recv.at[z], at(p, y)) for i, p in enumerate(z_peers)
     ]
-    for copy in zt_copies:
-        copy.start()
+    for copy in zt_copies[:-1]:
+        copy.start()
+
+    @pl.when(under)
+    def _():
+        pl.semaphore_wait(corner_in, 1)
+
+    zt_copies[-1].start()
 
     def after(p):
         return jnp.exp(sum(jnp.where(p < j, all_y[j], 0.0) for j in range(1, NY)))
@@ -193,6 +223,43 @@
             for j in range(nz)
         ]
 
+    def read_segments():
+        def add_later(j, total):
+            arrive(zt.at[j], zt_recv.at[j])
+            return total + zt[j]
+
+        later_z = lax.fori_loop(z + 1, nz, add_later, jnp.zeros_like(through))
+        weights = through * here * jnp.exp(later_z)
+        high, low = halves(weights)
+        packed[...] = jnp.concatenate([jnp.concatenate([high, low], axis=0)] * 2, axis=1)
+        parts = [None] * units
+        for s in range(seqs):
+            got = dot(packed[...], split[s])
+            for h in range(heads):
+                u = h * seqs + s
+                lanes = slice(h * DK, (h + 1) * DK)
+                parts[u] = got[u:u + 1, lanes] + got[units + u:units + u + 1, lanes]
+        yr[y] = jnp.concatenate(parts, axis=0)
+        yr_copies = [
+            remote(yr.at[y], yr.at[y], yr_send, yr_recv, at(z, p)) for i, p in enumerate(y_peers)
+        ]
+        for copy in yr_copies:
+            copy.start()
+
+
+    def share_read():
+        arrive(yr.at[0:NY - 1], yr_recv)
+        rz[z] = (yr[0] + yr[1]) + (yr[2] + yr[3])
+        rz_copies = [
+            remote(rz.at[z], rz.at[z], rz_send, rz_recv, at(p, y)) for i, p in enumerate(z_peers)
+        ]
+        for copy in rz_copies:
+            copy.start()
+
+
+    top, bottom = z == nz - 1, z == 0
+    pl.when(top)(read_segments)
+
     r2_copies = []
     for s in range(seqs):
         mine, theirs = near_scale(second[s], 0, s), near_scale(second[s], 1 + s % 2, s)
@@ -202,6 +269,9 @@
         copy = remote(q2.at[s], r2.at[s], r2_send, r2_recv.at[s], at(z, second[s]))
         copy.start()
         r2_copies.append(copy)
+
+    pl.when(bottom)(read_segments)
+    pl.when(top)(share_read)
 
     zr_copies = []
     for s in range(seqs):
@@ -216,35 +286,8 @@
             zr_copies.append(copy)
         zr[z, s] = zs[s, z]
 
-    def add_later(j, total):
-        arrive(zt.at[j], zt_recv.at[j])
-        return total + zt[j]
-
-    later_z = lax.fori_loop(z + 1, nz, add_later, jnp.zeros_like(through))
-    weights = through * here * jnp.exp(later_z)
-    high, low = halves(weights)
-    packed[...] = jnp.concatenate([jnp.concatenate([high, low], axis=0)] * 2, axis=1)
-    parts = [None] * units
-    for s in range(seqs):
-        got = dot(packed[...], split[s])
-        for h in range(heads):
-            u = h * seqs + s
-            lanes = slice(h * DK, (h + 1) * DK)
-            parts[u] = got[u:u + 1, lanes] + got[units + u:units + u + 1, lanes]
-    yr[y] = jnp.concatenate(parts, axis=0)
-    yr_copies = [
-        remote(yr.at[y], yr.at[y], yr_send, yr_recv, at(z, p)) for i, p in enumerate(y_peers)
-    ]
-    for copy in yr_copies:
-        copy.start()
-
-    arrive(yr.at[0:NY - 1], yr_recv)
-    rz[z] = (yr[0] + yr[1]) + (yr[2] + yr[3])
-    rz_copies = [
-        remote(rz.at[z], rz.at[z], rz_send, rz_recv, at(p, y)) for i, p in enumerate(z_peers)
-    ]
-    for copy in rz_copies:
-        copy.start()
+    pl.when(jnp.logical_not(top | bottom))(read_segments)
+    pl.when(jnp.logical_not(top))(share_read)
 
     def await_rest(j, carry):
         arrive(zt.at[j], zt_recv.at[j])
@@ -338,6 +381,7 @@
             pltpu.VMEM((4 * units, DK), F32),
             dma((CHUNKS,)),
             dma((4,)),
+            pltpu.SemaphoreType.REGULAR,
             dma,
             dma,
             dma,

time: 36.1 us -> 32.4 us (0.90)
  the two profiles are of different devices: /device:TPU:8 before, /device:TPU:6 now
where the time goes in v3:
time: 32.4 us; the launch traced here: 31.9 us
  Pallas kernels  30.1 us (93%)
  local copies, waits for them, and re-layouts  1.18 us (4%)
  between operations  0.64 us (2%)
    pallas_call x1, Pallas kernels, local(): pl.pallas_call(functools.partial(kernel, nz), out_shape=(pltpu.VMEM((seqs...  30.1 us
    unnamed x2, local copies, waits for them, and re-layouts  1.18 us

profile of v3, /device:TPU:6, one launch (start us, length us, event | category | flops | bytes accessed | tf_op | source)
XLA Modules:
  0.0 31.9 jit_solution(2243505437740627027)
XLA Ops:
  0.6 30.1 %shard_map.86 = (bf16[4,8,128]{2,1,0:T(8,128)(2,1)S(1)}, bf16[4,256]{1,0:T(4,128)(2,1)S(1)}) custom-call(bf16[512,4096]{1,0:T(8,128)(2,1)} %bitcast.5, bf16[4096,256]{1,0:T(8,128)(2,1)} %fw.1, bf16[4096,256]{1,0:T(8,128)(2,1)} %vw.1, f32[1,256]{1,0:T(1,128)} %bitcast.6, bf16[4,256]{1,0:T(4,128)(2,1)} %query_in.1, bf16[4,4096]{1,0:T(4,128)(2,1)} %next_in.1, ...), custom_call_target="tpu_custom_call" | custom-call | tf_op jit(solution)/shard_map/pallas_call | solution.py:348
  30.7 0.6 %copy.11 = bf16[4,2,4,128]{3,2,1,0:T(4,128)(2,1)} copy(bf16[4,2,4,128]{3,2,1,0:T(4,128)(2,1)S(1)} %bitcast.4) | data formatting | bytes 16384
  31.3 0.6 %copy.12 = bf16[4,256]{1,0:T(4,128)(2,1)} copy(bf16[4,256]{1,0:T(4,128)(2,1)S(1)} %get-tuple-element.7) | data formatting | bytes 4096

commit v4 on v3

--- a/solution.py
+++ b/solution.py
@@ -29,9 +29,9 @@
 def kernel(
     nz, prompt, fw, vw, leak_in, query_in, next_in, gain_in, cache_out, read_out,
     x, w, leak, query, nexts, gain, acc, inflow, decays, packed,
-    ys, split, r1, q2, r2, zs, zr, yt, zt, yr, rz, cols, cols_src, near, near_src,
+    ys, split, r1, q2, r2, zs, zr, yt, ct, lt, zt, yr, rz, cols, cols_src, near, near_src,
     load_sem, small_sem, corner_in,
-    yt_send, yt_recv, zt_send, zt_recv, r1_send, r1_recv, r2_send, r2_recv,
+    yt_send, yt_recv, ct_send, ct_recv, lt_send, lt_recv, zt_send, zt_recv, r1_send, r1_recv, r2_send, r2_recv,
     zr_send, zr_recv, yr_send, yr_recv, rz_send, rz_recv,
 ):
     seqs = query.shape[0]
@@ -48,8 +48,7 @@
         return {"sp": zz * NY + yy}
 
     y_peers = [lax.rem(y + d, NY) for d in range(1, NY)]
-    z_peers = [1 + lax.rem(z + i - 1, nz - 1) for i in range(1, nz - 1)]
-    z_peers.append((nz - 1) * lax.div(nz - z, nz))
+    z_peers = [i + lax.div(i - z + nz, nz) for i in range(nz - 1)]
 
     barrier = pltpu.get_barrier_semaphore()
     for p in y_peers:
@@ -136,6 +135,8 @@
     ]
     for copy in yt_copies:
         copy.start()
+    for j in range(1, nz - 1):
+        pl.when(z > j)(remote(yt.at[y], ct.at[z], ct_send, ct_recv.at[z], at(j, y)).start)
 
     rows_at = lax.broadcasted_iota(jnp.int32, (span, 2 * span), 0)
     cols_at = lax.rem(lax.broadcasted_iota(jnp.int32, (span, 2 * span), 1), span)
@@ -194,14 +195,15 @@
     zt_copies = [
         remote(zt.at[z], zt.at[z], zt_send, zt_recv.at[z], at(p, y)) for i, p in enumerate(z_peers)
     ]
-    for copy in zt_copies[:-1]:
+    pl.when(jnp.logical_not(under))(zt_copies[0].start)
+    for copy in zt_copies[1:]:
         copy.start()
 
     @pl.when(under)
     def _():
         pl.semaphore_wait(corner_in, 1)
-
-    zt_copies[-1].start()
+        zt_copies[0].start()
+
 
     def after(p):
         return jnp.exp(sum(jnp.where(p < j, all_y[j], 0.0) for j in range(1, NY)))
@@ -223,12 +225,7 @@
             for j in range(nz)
         ]
 
-    def read_segments():
-        def add_later(j, total):
-            arrive(zt.at[j], zt_recv.at[j])
-            return total + zt[j]
-
-        later_z = lax.fori_loop(z + 1, nz, add_later, jnp.zeros_like(through))
+    def read_segments(later_z):
         weights = through * here * jnp.exp(later_z)
         high, low = halves(weights)
         packed[...] = jnp.concatenate([jnp.concatenate([high, low], axis=0)] * 2, axis=1)
@@ -239,26 +236,29 @@
                 u = h * seqs + s
                 lanes = slice(h * DK, (h + 1) * DK)
                 parts[u] = got[u:u + 1, lanes] + got[units + u:units + u + 1, lanes]
-        yr[y] = jnp.concatenate(parts, axis=0)
-        yr_copies = [
-            remote(yr.at[y], yr.at[y], yr_send, yr_recv, at(z, p)) for i, p in enumerate(y_peers)
-        ]
-        for copy in yr_copies:
-            copy.start()
-
-
-    def share_read():
-        arrive(yr.at[0:NY - 1], yr_recv)
-        rz[z] = (yr[0] + yr[1]) + (yr[2] + yr[3])
-        rz_copies = [
-            remote(rz.at[z], rz.at[z], rz_send, rz_recv, at(p, y)) for i, p in enumerate(z_peers)
-        ]
-        for copy in rz_copies:
-            copy.start()
-
-
-    top, bottom = z == nz - 1, z == 0
-    pl.when(top)(read_segments)
+        rz[z] = jnp.concatenate(parts, axis=0)
+        for p in z_peers:
+            remote(rz.at[z], rz.at[z], rz_send, rz_recv, at(p, y)).start()
+
+    def add_arrived(totals, sems):
+        def add(j, total):
+            arrive(totals.at[j], sems.at[j])
+            return total + totals[j]
+
+        return lax.fori_loop(z + 1, nz, add, jnp.zeros_like(through))
+
+    def share_later():
+        lt[y] = add_arrived(ct, ct_recv)
+        for p in y_peers:
+            remote(lt.at[y], lt.at[y], lt_send, lt_recv, at(z, p)).start()
+
+    top, upper_half, inner = z == nz - 1, z >= nz // 2, (z > 0) & (z < nz - 1)
+
+    @pl.when(top)
+    def _():
+        read_segments(jnp.zeros_like(through))
+
+    pl.when(inner & upper_half)(share_later)
 
     r2_copies = []
     for s in range(seqs):
@@ -270,30 +270,41 @@
         copy.start()
         r2_copies.append(copy)
 
-    pl.when(bottom)(read_segments)
-    pl.when(top)(share_read)
-
-    zr_copies = []
+    pl.when(inner & jnp.logical_not(upper_half))(share_later)
+
+    @pl.when(inner)
+    def _():
+        arrive(lt.at[0:NY - 1], lt_recv)
+        read_segments((lt[0] + lt[1]) + (lt[2] + lt[3]))
+
+    @pl.when(z == 0)
+    def _():
+        read_segments(add_arrived(zt, zt_recv))
+
     for s in range(seqs):
         mine, theirs = near_scale(y, 0, s), near_scale(y, 1 + s % 2, s)
         near_copies[s].wait_recv()
         r2_copies[s].wait_recv()
         for j in range(nz):
-            zs[s, j] = (mine[j] * ys[y, s, j] + theirs[j] * r1[s, 0, j]) + r2[s, j]
-        for i, p in enumerate(z_peers):
-            copy = remote(zs.at[s, p], zr.at[z, s], zr_send, zr_recv.at[s], at(p, y))
-            copy.start()
-            zr_copies.append(copy)
-        zr[z, s] = zs[s, z]
-
-    pl.when(jnp.logical_not(top | bottom))(read_segments)
-    pl.when(jnp.logical_not(top))(share_read)
+            zs[j, s] = (mine[j] * ys[y, s, j] + theirs[j] * r1[s, 0, j]) + r2[s, j]
+        zr[z, s] = zs[z, s]
+
+    def send_state(p):
+        remote(zs.at[p], zr.at[z], zr_send, zr_recv, at(p, y)).start()
+
+    for p in z_peers:
+        send_state(p)
 
     def await_rest(j, carry):
         arrive(zt.at[j], zt_recv.at[j])
         return carry
 
     lax.fori_loop(0, z, await_rest, 0)
+
+    @pl.when(z > 0)
+    def _():
+        lax.fori_loop(z + 1, nz, await_rest, 0)
+
     running = jnp.zeros_like(through)
     for j in reversed(range(nz)):
         cols_src[j * units:(j + 1) * units, :] = jnp.exp(running)
@@ -305,18 +316,23 @@
         return spread(mine, [j * units + h * seqs + s for h in range(heads)])
 
     scale = [[column(j, s) for s in range(seqs)] for j in range(nz)]
-    for s in range(seqs):
-        arrive(zr.at[0:nz - 1, s], zr_recv.at[s])
+    arrive(rz.at[0:nz - 1], rz_recv)
+    column_read = rz[0]
+    for j in range(1, nz):
+        column_read = column_read + rz[j]
+    yr[y] = column_read
+    for p in y_peers:
+        remote(yr.at[y], yr.at[y], yr_send, yr_recv, at(z, p)).start()
+
+    arrive(zr.at[0:nz - 1], zr_recv)
     for s in range(seqs):
         total = scale[0][s] * zr[0, s]
         for j in range(1, nz):
             total = total + scale[j][s] * zr[j, s]
         cache_out[s] = total.astype(BF16)
 
-    arrive(rz.at[0:nz - 1], rz_recv)
-    raw = direct
-    for j in range(nz):
-        raw = raw + rz[j]
+    arrive(yr.at[0:NY - 1], yr_recv)
+    raw = direct + ((yr[0] + yr[1]) + (yr[2] + yr[3]))
     gain_row = gain[...]
     gains = jnp.concatenate(
         [jnp.broadcast_to(gain_row[:, h * DV:(h + 1) * DV], (seqs, DV)) for h in range(heads)], axis=0
@@ -327,6 +343,17 @@
     ).astype(BF16)
 
     arrive(yt.at[0:NY - 1], yt_send)
+
+    def await_sent(j, carry):
+        arrive(ct.at[0], ct_send)
+        return carry
+
+    lax.fori_loop(1, z, await_sent, 0)
+
+    @pl.when(inner)
+    def _():
+        arrive(lt.at[0:NY - 1], lt_send)
+
     arrive(zt.at[0:nz - 1], zt_send)
     for i in range(2):
         arrive(r1.at[:, i], r1_send)
@@ -369,8 +396,10 @@
             pltpu.VMEM((seqs, 2, nz, heads * own, DV), F32),
             pltpu.VMEM((seqs, nz, heads * own, DV), F32),
             pltpu.VMEM((seqs, nz, heads * own, DV), F32),
-            pltpu.VMEM((seqs, nz, heads * own, DV), F32),
             pltpu.VMEM((nz, seqs, heads * own, DV), F32),
+            pltpu.VMEM((nz, seqs, heads * own, DV), F32),
+            pltpu.VMEM((NY, units, DK), F32),
+            pltpu.VMEM((nz, units, DK), F32),
             pltpu.VMEM((NY, units, DK), F32),
             pltpu.VMEM((nz, units, DK), F32),
             pltpu.VMEM((NY, units, DV), F32),
@@ -387,11 +416,15 @@
             dma,
             dma((nz,)),
             dma,
+            dma,
+            dma,
+            dma((nz,)),
+            dma,
             dma((seqs, 2)),
             dma,
             dma((seqs,)),
             dma,
-            dma((seqs,)),
+            dma,
             dma,
             dma,
             dma,

time: 32.4 us -> 31.7 us (0.978); the launches traced: 31.9 us -> 31.5 us
  Pallas kernels: 30.1 us -> 29.7 us
    pallas_call x1, Pallas kernels: 30.1 us -> 29.7 us  [local(): pl.pallas_call(functools.partial(kernel, nz), out_shape=(pltpu.VMEM((seqs...]
where the time goes in v4:
time: 31.7 us; the launch traced here: 31.5 us
  Pallas kernels  29.7 us (94%)
  local copies, waits for them, and re-layouts  1.18 us (4%)
  between operations  0.64 us (2%)
    pallas_call x1, Pallas kernels, local(): pl.pallas_call(functools.partial(kernel, nz), out_shape=(pltpu.VMEM((seqs...  29.7 us
    unnamed x2, local copies, waits for them, and re-layouts  1.18 us

profile of v4, /device:TPU:6, one launch (start us, length us, event | category | flops | bytes accessed | tf_op | source)
XLA Modules:
  0.0 31.5 jit_solution(2611445143692600243)
XLA Ops:
  0.6 29.7 %shard_map.86 = (bf16[4,8,128]{2,1,0:T(8,128)(2,1)S(1)}, bf16[4,256]{1,0:T(4,128)(2,1)S(1)}) custom-call(bf16[512,4096]{1,0:T(8,128)(2,1)} %bitcast.5, bf16[4096,256]{1,0:T(8,128)(2,1)} %fw.1, bf16[4096,256]{1,0:T(8,128)(2,1)} %vw.1, f32[1,256]{1,0:T(1,128)} %bitcast.6, bf16[4,256]{1,0:T(4,128)(2,1)} %query_in.1, bf16[4,4096]{1,0:T(4,128)(2,1)} %next_in.1, ...), custom_call_target="tpu_custom_call" | custom-call | tf_op jit(solution)/shard_map/pallas_call | solution.py:375
  30.4 0.6 %copy.11 = bf16[4,2,4,128]{3,2,1,0:T(4,128)(2,1)} copy(bf16[4,2,4,128]{3,2,1,0:T(4,128)(2,1)S(1)} %bitcast.4) | data formatting | bytes 16384
  31.0 0.6 %copy.12 = bf16[4,256]{1,0:T(4,128)(2,1)} copy(bf16[4,256]{1,0:T(4,128)(2,1)S(1)} %get-tuple-element.7) | data formatting | bytes 4096

commit v5 on v4

--- a/solution.py
+++ b/solution.py
@@ -31,8 +31,7 @@
     x, w, leak, query, nexts, gain, acc, inflow, decays, packed,
     ys, split, r1, q2, r2, zs, zr, yt, ct, lt, zt, yr, rz, cols, cols_src, near, near_src,
     load_sem, small_sem, corner_in,
-    yt_send, yt_recv, ct_send, ct_recv, lt_send, lt_recv, zt_send, zt_recv, r1_send, r1_recv, r2_send, r2_recv,
-    zr_send, zr_recv, yr_send, yr_recv, rz_send, rz_recv,
+    sent, yt_recv, ct_recv, lt_recv, zt_recv, r1_recv, r2_recv, zr_recv, yr_recv, rz_recv,
 ):
     seqs = query.shape[0]
     span = x.shape[0] // seqs
@@ -49,15 +48,6 @@
 
     y_peers = [lax.rem(y + d, NY) for d in range(1, NY)]
     z_peers = [i + lax.div(i - z + nz, nz) for i in range(nz - 1)]
-
-    barrier = pltpu.get_barrier_semaphore()
-    for p in y_peers:
-        pl.semaphore_signal(barrier, inc=1, device_id=at(z, p), device_id_type=MESH)
-
-    @pl.when(me > 0)
-    def _():
-        for p in z_peers:
-            pl.semaphore_signal(barrier, inc=1, device_id=at(p, y), device_id_type=MESH)
 
     def cut(c):
         return pl.ds(c * step, step)
@@ -76,6 +66,15 @@
     for copy in small:
         copy.start()
 
+    barrier = pltpu.get_barrier_semaphore()
+    for p in y_peers:
+        pl.semaphore_signal(barrier, inc=1, device_id=at(z, p), device_id_type=MESH)
+
+    @pl.when(me > 0)
+    def _():
+        for p in z_peers:
+            pl.semaphore_signal(barrier, inc=1, device_id=at(p, y), device_id_type=MESH)
+
     def greet_column():
         pl.semaphore_wait(barrier, NY - 1 + nz - 1)
         for p in z_peers:
@@ -131,12 +130,12 @@
         pl.semaphore_wait(barrier, NY - 1 + nz - 1)
 
     yt_copies = [
-        remote(yt.at[y], yt.at[y], yt_send, yt_recv, at(z, p)) for i, p in enumerate(y_peers)
+        remote(yt.at[y], yt.at[y], sent, yt_recv, at(z, p)) for i, p in enumerate(y_peers)
     ]
     for copy in yt_copies:
         copy.start()
     for j in range(1, nz - 1):
-        pl.when(z > j)(remote(yt.at[y], ct.at[z], ct_send, ct_recv.at[z], at(j, y)).start)
+        pl.when(z > j)(remote(yt.at[y], ct.at[z], sent, ct_recv.at[z], at(j, y)).start)
 
     rows_at = lax.broadcasted_iota(jnp.int32, (span, 2 * span), 0)
     cols_at = lax.rem(lax.broadcasted_iota(jnp.int32, (span, 2 * span), 1), span)
@@ -169,12 +168,12 @@
     for s in range(seqs):
         p = first[s]
         beyond = NY - 1 - p if s % 2 == 0 else p + 1 - 2 * lax.rem(p, 2)
-        copy = remote(ys.at[beyond, s], r1.at[s, 1], r1_send, r1_recv.at[s, 1], at(z, p))
+        copy = remote(ys.at[beyond, s], r1.at[s, 1], sent, r1_recv.at[s], at(z, p))
         copy.start()
         far_copies.append(copy)
     for s in range(seqs):
         p = first[s]
-        copy = remote(ys.at[p, s], r1.at[s, 0], r1_send, r1_recv.at[s, 0], at(z, p))
+        copy = remote(ys.at[p, s], r1.at[s, 0], sent, r2_recv.at[s], at(z, p))
         copy.start()
         near_copies.append(copy)
 
@@ -193,7 +192,7 @@
     all_y = [yt[j] for j in range(NY)]
     zt[z] = sum(all_y[1:], all_y[0])
     zt_copies = [
-        remote(zt.at[z], zt.at[z], zt_send, zt_recv.at[z], at(p, y)) for i, p in enumerate(z_peers)
+        remote(zt.at[z], zt.at[z], sent, zt_recv.at[z], at(p, y)) for i, p in enumerate(z_peers)
     ]
     pl.when(jnp.logical_not(under))(zt_copies[0].start)
     for copy in zt_copies[1:]:
@@ -238,7 +237,7 @@
                 parts[u] = got[u:u + 1, lanes] + got[units + u:units + u + 1, lanes]
         rz[z] = jnp.concatenate(parts, axis=0)
         for p in z_peers:
-            remote(rz.at[z], rz.at[z], rz_send, rz_recv, at(p, y)).start()
+            remote(rz.at[z], rz.at[z], sent, rz_recv, at(p, y)).start()
 
     def add_arrived(totals, sems):
         def add(j, total):
@@ -250,7 +249,7 @@
     def share_later():
         lt[y] = add_arrived(ct, ct_recv)
         for p in y_peers:
-            remote(lt.at[y], lt.at[y], lt_send, lt_recv, at(z, p)).start()
+            remote(lt.at[y], lt.at[y], sent, lt_recv, at(z, p)).start()
 
     top, upper_half, inner = z == nz - 1, z >= nz // 2, (z > 0) & (z < nz - 1)
 
@@ -266,11 +265,27 @@
         far_copies[s].wait_recv()
         for j in range(nz):
             q2[s, j] = mine[j] * ys[second[s], s, j] + theirs[j] * r1[s, 1, j]
-        copy = remote(q2.at[s], r2.at[s], r2_send, r2_recv.at[s], at(z, second[s]))
+        copy = remote(q2.at[s], r2.at[s], sent, r2_recv.at[s], at(z, second[s]))
         copy.start()
         r2_copies.append(copy)
 
     pl.when(inner & jnp.logical_not(upper_half))(share_later)
+
+    def send_state(p):
+        remote(zs.at[p], zr.at[z], sent, zr_recv, at(p, y)).start()
+
+    def prepare_states():
+        for s in range(seqs):
+            mine, theirs = near_scale(y, 0, s), near_scale(y, 1 + s % 2, s)
+            arrive(r1.at[s], r2_recv.at[s])
+            for j in range(nz):
+                zs[j, s] = (mine[j] * ys[y, s, j] + theirs[j] * r1[s, 0, j]) + r2[s, j]
+            zr[z, s] = zs[z, s]
+        for p in z_peers[:2]:
+            send_state(p)
+
+    soon = (z > 0) & (z < nz // 2)
+    pl.when(soon)(prepare_states)
 
     @pl.when(inner)
     def _():
@@ -281,18 +296,8 @@
     def _():
         read_segments(add_arrived(zt, zt_recv))
 
-    for s in range(seqs):
-        mine, theirs = near_scale(y, 0, s), near_scale(y, 1 + s % 2, s)
-        near_copies[s].wait_recv()
-        r2_copies[s].wait_recv()
-        for j in range(nz):
-            zs[j, s] = (mine[j] * ys[y, s, j] + theirs[j] * r1[s, 0, j]) + r2[s, j]
-        zr[z, s] = zs[z, s]
-
-    def send_state(p):
-        remote(zs.at[p], zr.at[z], zr_send, zr_recv, at(p, y)).start()
-
-    for p in z_peers:
+    pl.when(jnp.logical_not(soon))(prepare_states)
+    for p in z_peers[2:]:
         send_state(p)
 
     def await_rest(j, carry):
@@ -322,7 +327,7 @@
         column_read = column_read + rz[j]
     yr[y] = column_read
     for p in y_peers:
-        remote(yr.at[y], yr.at[y], yr_send, yr_recv, at(z, p)).start()
+        remote(yr.at[y], yr.at[y], sent, yr_recv, at(z, p)).start()
 
     arrive(zr.at[0:nz - 1], zr_recv)
     for s in range(seqs):
@@ -342,25 +347,25 @@
         [normed[h * seqs:(h + 1) * seqs, :] for h in range(heads)], axis=1
     ).astype(BF16)
 
-    arrive(yt.at[0:NY - 1], yt_send)
+    arrive(yt.at[0:NY - 1], sent)
 
     def await_sent(j, carry):
-        arrive(ct.at[0], ct_send)
+        arrive(ct.at[0], sent)
         return carry
 
     lax.fori_loop(1, z, await_sent, 0)
 
     @pl.when(inner)
     def _():
-        arrive(lt.at[0:NY - 1], lt_send)
-
-    arrive(zt.at[0:nz - 1], zt_send)
+        arrive(lt.at[0:NY - 1], sent)
+
+    arrive(zt.at[0:nz - 1], sent)
     for i in range(2):
-        arrive(r1.at[:, i], r1_send)
-    arrive(r2, r2_send)
-    arrive(zr.at[0:nz - 1], zr_send)
-    arrive(yr.at[0:NY - 1], yr_send)
-    arrive(rz.at[0:nz - 1], rz_send)
+        arrive(r1.at[:, i], sent)
+    arrive(r2, sent)
+    arrive(zr.at[0:nz - 1], sent)
+    arrive(yr.at[0:NY - 1], sent)
+    arrive(rz.at[0:nz - 1], sent)
 
 
 def local(prompt, forget_weight, value_weight, leak, query, next_input, read_gain):
@@ -413,19 +418,11 @@
             pltpu.SemaphoreType.REGULAR,
             dma,
             dma,
-            dma,
             dma((nz,)),
             dma,
-            dma,
-            dma,
             dma((nz,)),
-            dma,
-            dma((seqs, 2)),
-            dma,
             dma((seqs,)),
-            dma,
-            dma,
-            dma,
+            dma((seqs,)),
             dma,
             dma,
             dma,

time: 31.7 us -> 31.7 us (level)
  no operation moved by 1% of the time
where the time goes in v5:
time: 31.7 us; the launch traced here: 31.5 us
  Pallas kernels  29.7 us (94%)
  local copies, waits for them, and re-layouts  1.18 us (4%)
  between operations  0.64 us (2%)
    pallas_call x1, Pallas kernels, local(): pl.pallas_call(functools.partial(kernel, nz), out_shape=(pltpu.VMEM((seqs...  29.7 us
    unnamed x2, local copies, waits for them, and re-layouts  1.18 us

profile of v5, /device:TPU:6, one launch (start us, length us, event | category | flops | bytes accessed | tf_op | source)
XLA Modules:
  0.0 31.5 jit_solution(4270090493313482724)
XLA Ops:
  0.6 29.7 %shard_map.86 = (bf16[4,8,128]{2,1,0:T(8,128)(2,1)S(1)}, bf16[4,256]{1,0:T(4,128)(2,1)S(1)}) custom-call(bf16[512,4096]{1,0:T(8,128)(2,1)} %bitcast.5, bf16[4096,256]{1,0:T(8,128)(2,1)} %fw.1, bf16[4096,256]{1,0:T(8,128)(2,1)} %vw.1, f32[1,256]{1,0:T(1,128)} %bitcast.6, bf16[4,256]{1,0:T(4,128)(2,1)} %query_in.1, bf16[4,4096]{1,0:T(4,128)(2,1)} %next_in.1, ...), custom_call_target="tpu_custom_call" | custom-call | tf_op jit(solution)/shard_map/pallas_call | solution.py:380
  30.3 0.6 %copy.11 = bf16[4,2,4,128]{3,2,1,0:T(4,128)(2,1)} copy(bf16[4,2,4,128]{3,2,1,0:T(4,128)(2,1)S(1)} %bitcast.4) | data formatting | bytes 16384
  30.9 0.6 %copy.12 = bf16[4,256]{1,0:T(4,128)(2,1)} copy(bf16[4,256]{1,0:T(4,128)(2,1)S(1)} %get-tuple-element.7) | data formatting | bytes 4096
